TPU v7x, 32 devices: a whole 2x2x4 slice. The times are simulated.
32 devices in a mesh: sp: 8 (over z, y), tp: 4 (over x, core).
Axes of the slice: x: 2, y: 2, z: 4, core: 2. Of those that a mesh axis runs over, the one named last changes fastest.
Arguments:
- stream_in: bfloat16 [6144, 2048], P(('sp', 'tp')), may hold values from -6 to 6
- query_wide: bfloat16 [6144, 512], P('sp', 'tp'), may hold values from -6 to 6
- key_wide: bfloat16 [6144, 512], P('sp', 'tp'), may hold values from -6 to 6
- value_wide: bfloat16 [6144, 512], P('sp', 'tp'), may hold values from -6 to 6
- gate_wide: bfloat16 [6144, 512], P('sp', 'tp'), may hold values from -6 to 6
- decay_wide: float32 [4, 6144], P('tp', 'sp'), may hold values from -2.3 to 0, as said below
- query_narrow: bfloat16 [6144, 512], P('sp', 'tp'), may hold values from -6 to 6
- key_narrow: bfloat16 [6144, 512], P('sp', 'tp'), may hold values from -6 to 6
- value_narrow: bfloat16 [6144, 512], P('sp', 'tp'), may hold values from -6 to 6
- gate_narrow: bfloat16 [6144, 512], P('sp', 'tp'), may hold values from -6 to 6
- decay_narrow: float32 [8, 6144], P('tp', 'sp'), may hold values from -2.3 to 0, as said below
- output_wide: bfloat16 [512, 2048], P('tp'), may hold values from -0.25 to 0.25
- output_narrow: bfloat16 [512, 2048], P('tp'), may hold values from -0.25 to 0.25
- norm_gain: bfloat16 [2048], replicated, may hold values from 0.099609375 to 1.8984375
- up_weight: bfloat16 [2048, 8192], P('sp', 'tp'), may hold values from -0.125 to 0.125
- down_weight: bfloat16 [8192, 2048], P('tp', 'sp'), may hold values from -0.0625 to 0.0625
Outputs:
- layer_out: bfloat16 [6144, 2048], P(('sp', 'tp'))
Inputs may be any that keep to these rules, and one draw needn't show every extreme that they name: `decay_wide`: each entry is the logarithm of one head's retention factor at one position. `decay_narrow`: each entry is the logarithm of one head's retention factor at one position.
All inputs are finite; a program needn't handle non-finite values.
Results may differ from a plain program's by a relative error of at most 0.02.
Values may be sent and summed in bfloat16 or wider, within the bound.
A program may use at most 128 MiB of HBM per device.

v0:
```python
import jax
import jax.numpy as jnp
from jax import lax
from jax.sharding import PartitionSpec as P

HDW = 128
HDN = 64
BLOCK = 128
head_eps = 1e-05
norm_eps = 1e-06
rope_base = 10000.0


def carried_in(shard, axis, join, neutral):
    place = lax.axis_index(axis)
    gathered = jax.tree.map(
        lambda a, kind: lax.all_gather(a.astype(kind), axis),
        shard,
        (jnp.bfloat16, jnp.bfloat16, jnp.bfloat16, jnp.bfloat16),
    )
    state = jax.tree.map(lambda a, e: jnp.zeros_like(a) + jnp.asarray(e, a.dtype), shard, neutral)

    def one(turn, state):
        return join(
            state,
            jax.tree.map(
                lambda a, own: lax.dynamic_index_in_dim(a, turn, 0, False).astype(own.dtype),
                gathered,
                shard,
            ),
        )

    return lax.fori_loop(0, place, one, state)


def rotate(values, places):
    half = values.shape[-1] // 2
    inverse = rope_base ** (-jnp.arange(half, dtype=jnp.float32) / half)
    angles = places[:, None] * inverse[None, :]
    cosine = jnp.cos(angles)[:, None, :]
    sine = jnp.sin(angles)[:, None, :]
    front = values[..., :half]
    back = values[..., half:]
    return jnp.concatenate([front * cosine - back * sine, back * cosine + front * sine], axis=-1)


def block_step(carried, inputs):
    query, keys, values, log_rate = inputs
    running = jnp.cumsum(log_rate, axis=0)
    spread = running[:, None, :] - running[None, :, :]
    length = log_rate.shape[0]
    lower = (jnp.arange(length)[:, None] >= jnp.arange(length)[None, :])[:, :, None]
    factor = jnp.where(lower, jnp.exp(jnp.minimum(spread, 0.0)), 0.0)
    scores = jnp.einsum("thd,shd->tsh", query, keys) * factor
    within = jnp.einsum("tsh,she->the", scores, values)
    across = jnp.einsum("thd,hde->the", query, carried) * jnp.exp(running)[:, :, None]
    tail_decay = jnp.exp(running[-1][None, :] - running)
    updated = jnp.exp(running[-1])[:, None, None] * carried + jnp.einsum(
        "shd,she->hde", keys * tail_decay[:, :, None], values
    )
    return (updated, within + across)


def head_norm(values):
    centre = values - jnp.mean(values, axis=-1, keepdims=True)
    spread = jnp.mean(centre * centre, axis=-1, keepdims=True)
    return centre * lax.rsqrt(spread + head_eps)


def local_group(query, keys, values, log_rate, width, places):
    length = query.shape[0]
    count_of_heads = query.shape[1] // width
    blocks = length // BLOCK

    def split(array):
        return array.astype(jnp.float32).reshape(length, count_of_heads, width)

    query_rot = rotate(split(query), places)
    keys_rot = rotate(split(keys), places) * width ** (-0.5)
    rates = log_rate.T
    carried = jnp.zeros((count_of_heads, width, width), jnp.float32)
    final_state, outputs = lax.scan(
        block_step,
        carried,
        (
            query_rot.reshape(blocks, BLOCK, count_of_heads, width),
            keys_rot.reshape(blocks, BLOCK, count_of_heads, width),
            split(values).reshape(blocks, BLOCK, count_of_heads, width),
            rates.reshape(blocks, BLOCK, count_of_heads),
        ),
    )
    running = jnp.cumsum(rates, axis=0)
    return (
        query_rot,
        outputs.reshape(length, count_of_heads, width),
        final_state,
        jnp.exp(running[-1]),
        running,
    )


def finish_group(query_rot, outputs, incoming, running, gate):
    length = outputs.shape[0]
    outputs = (
        outputs + jnp.einsum("thd,hde->the", query_rot, incoming) * jnp.exp(running)[:, :, None]
    )
    normed = head_norm(outputs).reshape(length, -1)
    return (jax.nn.silu(gate.astype(jnp.float32)) * normed).astype(jnp.bfloat16)


def chain(earlier, later):
    rate_wide, memory_wide, rate_narrow, memory_narrow = earlier
    later_rate_wide, later_memory_wide, later_rate_narrow, later_memory_narrow = later
    return (
        rate_wide * later_rate_wide,
        memory_wide * later_rate_wide[:, None, None] + later_memory_wide,
        rate_narrow * later_rate_narrow,
        memory_narrow * later_rate_narrow[:, None, None] + later_memory_narrow,
    )


def row_norm(middle, norm_gain):
    middle_f = middle.astype(jnp.float32)
    scale = lax.rsqrt(jnp.mean(middle_f * middle_f, axis=-1, keepdims=True) + norm_eps)
    return (middle_f * scale * norm_gain.astype(jnp.float32)).astype(jnp.bfloat16)


def on_device(
    stream_in,
    query_wide,
    key_wide,
    value_wide,
    gate_wide,
    decay_wide,
    query_narrow,
    key_narrow,
    value_narrow,
    gate_narrow,
    decay_narrow,
    output_wide,
    output_narrow,
    norm_gain,
    up_weight,
    down_weight,
):
    length = query_wide.shape[0]
    places = (lax.axis_index("sp") * length + jnp.arange(length, dtype=jnp.int32)).astype(
        jnp.float32
    )
    wide_query, wide_out, wide_state, wide_total, wide_running = local_group(
        query_wide, key_wide, value_wide, decay_wide, HDW, places
    )
    narrow_query, narrow_out, narrow_state, narrow_total, narrow_running = local_group(
        query_narrow, key_narrow, value_narrow, decay_narrow, HDN, places
    )
    identity = (
        jnp.ones_like(wide_total),
        jnp.zeros_like(wide_state),
        jnp.ones_like(narrow_total),
        jnp.zeros_like(narrow_state),
    )
    incoming = carried_in(
        (wide_total, wide_state, narrow_total, narrow_state), "sp", chain, identity
    )
    mixed_wide = finish_group(wide_query, wide_out, incoming[1], wide_running, gate_wide)
    mixed_narrow = finish_group(narrow_query, narrow_out, incoming[3], narrow_running, gate_narrow)
    mixed_sum = lax.psum_scatter(
        (
            jnp.dot(mixed_wide, output_wide, preferred_element_type=jnp.float32)
            + jnp.dot(mixed_narrow, output_narrow, preferred_element_type=jnp.float32)
        ).astype(jnp.bfloat16),
        "tp",
        scatter_dimension=0,
        tiled=True,
    ).astype(jnp.float32)
    middle = (stream_in.astype(jnp.float32) + mixed_sum).astype(jnp.bfloat16)
    normed = lax.all_gather(row_norm(middle, norm_gain), "tp", axis=0, tiled=True)
    up_sum = jnp.dot(
        normed,
        lax.all_gather(up_weight, "sp", axis=0, tiled=True),
        preferred_element_type=jnp.float32,
    )
    hidden = jnp.square(jax.nn.relu(up_sum)).astype(jnp.bfloat16)
    down_sum = jnp.dot(
        hidden,
        lax.all_gather(down_weight, "sp", axis=1, tiled=True),
        preferred_element_type=jnp.float32,
    )
    down_rows = lax.psum_scatter(
        down_sum.astype(jnp.bfloat16), "tp", scatter_dimension=0, tiled=True
    ).astype(jnp.float32)
    return (middle.astype(jnp.float32) + down_rows).astype(jnp.bfloat16)


def solution(mesh):
    in_specs = (
        P(("sp", "tp"), None),
        P("sp", "tp"),
        P("sp", "tp"),
        P("sp", "tp"),
        P("sp", "tp"),
        P("tp", "sp"),
        P("sp", "tp"),
        P("sp", "tp"),
        P("sp", "tp"),
        P("sp", "tp"),
        P("tp", "sp"),
        P("tp", None),
        P("tp", None),
        P(),
        P("sp", "tp"),
        P("tp", "sp"),
    )
    out_specs = P(("sp", "tp"), None)
    return jax.shard_map(
        on_device, mesh=mesh, in_specs=in_specs, out_specs=out_specs, check_vma=False
    )
```

profile of v0, /device:TPU:0, one launch (start us, length us, event | category | flops | bytes accessed | tf_op | source)
XLA Modules:
  0.0 578.7 jit_solution(15378131517314459082)
XLA Ops:
  6.6 0.8 reduce.3
  8.2 1.1 copy.75
  9.3 1.1 copy.77
  11.9 25.0 %while.43 = (s32[]{:T(128)}, f32[2,64,64]{2,1,0:T(8,128)S(1)}, f32[6,128,2,64]{1,0,3,2:T(8,128)}, f32[6,128,2]{2,1,0:T(8,128)S(1)}, f32[6,128,2,64]{1,0,3,2:T(8,...) while((s32[]{:T(128)}, f32[2,64,64]{2,1,0:T(8,128)S(1)}, ...), condition=%wide.region_9.10_spmd.clone, body=%wide.region_7.9_spmd.clone.sunk | while | flops 12877827 | bytes 1099440 | solution.py:82
  13.0 2.8 dynamic_update_slice.14
  17.2 2.8 dynamic_update_slice.14
  21.4 2.8 dynamic_update_slice.14
  25.5 2.8 dynamic_update_slice.14
  29.7 2.8 dynamic_update_slice.14
  33.8 2.8 dynamic_update_slice.14
  36.9 34.6 %all-gather.1 = bf16[16,64,64]{2,1,0:T(8,128)(2,1)} all-gather(bf16[2,64,64]{2,1,0:T(8,128)(2,1)S(1)} %convert_element_type.115), channel_id=3, replica_groups=mesh['sp'=8,'tp'=4] {'sp'}, dimensions={0}, use_global_device_ids=true | all-gather | bytes 147456 | tf_op jit(solution)/shard_map/all_gather | solution.py:17
  71.4 1.0 reshape_reshape.16
  72.4 1.0 bitcast_convert_fusion.1
  73.4 1.9 fusion.74
  75.4 0.9 maximum_multiply_fusion.1
  76.4 27.8 %while.42 = (s32[]{:T(128)}, f32[1,128,128]{2,1,0:T(8,128)S(1)}, f32[6,128,1,128]{3,1,0,2:T(8,128)}, f32[6,128,1]{1,2,0:T(1,128)}, f32[6,128,1,128]{3,2,1,0:T(1,...) while((s32[]{:T(128)}, f32[1,128,128]{2,1,0:T(8,128)S(1)}, ...), condition=%wide.region_2.3_spmd.clone, body=%wide.region_0.2_spmd.clone.sunk | while | flops 17006596 | bytes 1515172 | solution.py:82
  76.4 0.7 fusion.149
  78.0 0.6 fusion.150
  81.0 0.7 fusion.149
  82.6 0.6 fusion.150
  85.6 0.7 fusion.149
  87.2 0.6 fusion.150
  90.3 0.7 fusion.149
  91.9 0.6 fusion.150
  94.9 0.7 fusion.149
  96.5 0.6 fusion.150
  99.5 0.7 fusion.149
  101.1 0.6 fusion.150
  102.6 0.6 constant_dynamic-update-slice_fusion.2
  104.2 30.9 %all-gather = bf16[8,128,128]{2,1,0:T(8,128)(2,1)S(1)} all-gather(bf16[1,128,128]{2,1,0:T(8,128)(2,1)S(1)} %convert_element_type.113), channel_id=2, replica_groups=mesh['sp'=8,'tp'=4] {'sp'}, dimensions={0}, use_global_device_ids=true | all-gather | bytes 294912 | tf_op jit(solution)/shard_map/all_gather | solution.py:17
  135.7 0.6 slice.73
  138.3 0.7 dynamic-update-slice
  139.0 21.4 %all-reduce = bf16[8]{0:T(256)(128)(2,1)S(1)} all-reduce(bf16[8]{0:T(256)(128)(2,1)S(1)} %dynamic-update-slice), channel_id=1, replica_groups=mesh['sp'=8,'tp'=4] {'sp'}, use_global_device_ids=true, to_apply=%add | all-reduce | flops 8 | bytes 32
  161.6 16.3 %all-gather.2 = bf16[8,1,2]{2,1,0:T(2,128)(2,1)S(1)} all-gather(bf16[1,1,2]{2,1,0:T(2,128)(2,1)S(1)} %bitcast.321), channel_id=1, replica_groups=mesh['sp'=8,'tp'=4] {'sp'}, dimensions={0}, use_global_device_ids=true | all-gather | bytes 36 | tf_op jit(solution)/shard_map/all_gather | solution.py:17
  178.0 1.2 reshape.610
  180.7 1.0 fusion.79
  181.7 2.7 add_convert_fusion
  185.1 52.4 %reduce-scatter.3.cloned.1.call-done = bf16[192,2048]{1,0:T(8,128)(2,1)} async-done(((bf16[768,2048]{1,0:T(8,128)(2,1)}), bf16[192,2048]{1,0:T(8,128)(2,1)}) %reduce-scatter.3.cloned.1.call-update) | async-done | bytes 786448 | tf_op jit(solution)/shard_map/reduce_scatter | solution.py:167
  237.5 1.5 fusion.47
  239.0 2.3 fusion.49
  241.4 0.7 all-gather.9.cloned.1.call-update
  242.9 27.1 %all-gather.7.cloned.1.call-done = bf16[768,2048]{1,0:T(8,128)(2,1)} async-done(((bf16[192,2048]{1,0:T(8,128)(2,1)}), bf16[768,2048]{1,0:T(8,128)(2,1)}) %all-gather.7.cloned.1.call-update) | async-done | bytes 3145744 | tf_op jit(solution)/shard_map/all_gather | solution.py:177
  270.0 126.6 %all-gather.9.cloned.1.call-done = bf16[2048,2048]{1,0:T(8,128)(2,1)} async-done(((bf16[256,2048]{1,0:T(8,128)(2,1)}), bf16[2048,2048]{1,0:T(8,128)(2,1)}) %all-gather.9.cloned.1.call-update) | async-done | bytes 8388624 | tf_op jit(solution)/shard_map/all_gather | solution.py:180
  396.7 11.9 %multiply_convert_fusion = bf16[768,2048]{1,0:T(8,128)(2,1)} fusion(bf16[768,2048]{1,0:T(8,128)(2,1)} %all-gather.7.cloned.1.call-done, bf16[2048,2048]{1,0:T(8,128)(2,1)} %all-gather.9.cloned.1.call-done), kind=kOutput, calls=%fused_computation.73 | convolution fusion | flops 6447169536 | bytes 14680064 | tf_op jit(solution)/shard_map/dot_general | solution.py:178
  408.5 113.2 %all-gather.11.cloned.1.call-done = bf16[2048,2048]{1,0:T(8,128)(2,1)} async-done(((bf16[2048,256]{1,0:T(8,128)(2,1)}), bf16[2048,2048]{1,0:T(8,128)(2,1)}) %all-gather.11.cloned.1.call-update) | async-done | bytes 8388624 | tf_op jit(solution)/shard_map/all_gather | solution.py:186
  521.7 11.9 %convolution_convert_fusion = bf16[768,2048]{1,0:T(8,128)(2,1)} fusion(bf16[768,2048]{1,0:T(8,128)(2,1)} %multiply_convert_fusion, bf16[2048,2048]{1,0:T(8,128)(2,1)} %all-gather.11.cloned.1.call-done), kind=kOutput, calls=%fused_computation.75 | convolution fusion | flops 6444023808 | bytes 14680064 | tf_op jit(solution)/shard_map/dot_general | solution.py:184
  533.6 36.2 %reduce-scatter.5.cloned.1.call-done = bf16[192,2048]{1,0:T(8,128)(2,1)} async-done(((bf16[768,2048]{1,0:T(8,128)(2,1)}), bf16[192,2048]{1,0:T(8,128)(2,1)}) %reduce-scatter.5.cloned.1.call-update) | async-done | bytes 786448 | tf_op jit(solution)/shard_map/reduce_scatter | solution.py:189
  569.8 2.4 fusion.50
  (233 shorter events, 30.5 us)
Async XLA Ops:
  6.5 174.1 %copy-start = (bf16[128,2048]{1,0:T(8,128)(2,1)S(1)}, bf16[128,2048]{1,0:T(8,128)(2,1)}, u32[]{:S(2)}) copy-start(bf16[128,2048]{1,0:T(8,128)(2,1)} %param.33) | copy-start | bytes 1572868
  6.5 4.5 copy-start.8
  6.5 231.0 %reduce-scatter.3.cloned.1.call-start = ((), (), s32[]{:S(2)}) async-start(), calls=%async_computation.2 | async-start | bytes 3932160 | tf_op jit(solution)/shard_map/reduce_scatter | solution.py:167
  9.3 2.3 copy-start.9
  11.9 60.5 %copy-start.5 = (bf16[768,128]{1,0:T(8,128)(2,1)S(1)}, bf16[768,128]{1,0:T(8,128)(2,1)}, u32[]{:S(2)}) copy-start(bf16[768,128]{1,0:T(8,128)(2,1)} %param.23) | copy-start | bytes 589828
  76.4 61.3 %copy-start.11 = (u32[32]{0:T(128)S(1)}, u32[32]{0:T(128)}, u32[]{:S(2)}) copy-start(u32[32]{0:T(128)} %constant.123) | copy-start | bytes 388
  104.2 75.5 %copy-start.6 = (bf16[768,128]{1,0:T(8,128)(2,1)S(1)}, bf16[768,128]{1,0:T(8,128)(2,1)}, u32[]{:S(2)}) copy-start(bf16[768,128]{1,0:T(8,128)(2,1)} %param.31) | copy-start | bytes 589828
  104.2 75.6 %copy-start.4 = (f32[6,128,1,128]{3,1,0,2:T(8,128)S(1)}, f32[6,128,1,128]{3,1,0,2:T(8,128)}, u32[]{:S(2)}) copy-start(f32[6,128,1,128]{3,1,0,2:T(8,128)} %get-tuple-element.151) | copy-start | bytes 1179652
  178.0 2.4 copy-start.7
  180.7 1.0 copy-start.3
  184.4 0.7 copy-start.10
  184.4 53.1 %copy-start.1 = (bf16[192,2048]{1,0:T(8,128)(2,1)S(1)}, bf16[192,2048]{1,0:T(8,128)(2,1)}, u32[]{:S(2)}) copy-start(bf16[192,2048]{1,0:T(8,128)(2,1)} %param.22) | copy-start | bytes 2359300
  184.4 85.6 %all-gather.7.cloned.1.call-start = ((), (), s32[]{:S(2)}) async-start(), calls=%async_computation.3 | async-start | bytes 3932160 | tf_op jit(solution)/shard_map/all_gather | solution.py:177
  241.3 155.3 %all-gather.9.cloned.1.call-start = ((), (), s32[]{:S(2)}) async-start(), calls=%async_computation.4 | async-start | bytes 9437184 | tf_op jit(solution)/shard_map/all_gather | solution.py:180
  242.1 279.6 %all-gather.11.cloned.1.call-start = ((), (), s32[]{:S(2)}) async-start(), calls=%async_computation.5 | async-start | bytes 9437184 | tf_op jit(solution)/shard_map/all_gather | solution.py:186
  242.7 327.2 %reduce-scatter.5.cloned.1.call-start = ((), (), s32[]{:S(2)}) async-start(), calls=%async_computation.6 | async-start | bytes 3932160 | tf_op jit(solution)/shard_map/reduce_scatter | solution.py:189
  533.6 36.2 %copy-start.2 = (bf16[192,2048]{1,0:T(8,128)(2,1)S(1)}, bf16[192,2048]{1,0:T(8,128)(2,1)}, u32[]{:S(2)}) copy-start(bf16[192,2048]{1,0:T(8,128)(2,1)} %reduce-scatter.3.cloned.1.call-done) | copy-start | bytes 2359300
Sparse Core Ops, SparseCore 0:
  184.5 52.9 reduce-scatter.2
  241.5 28.5 all-gather.6
  272.1 124.4 all-gather.8
  398.6 123.1 all-gather.10
  533.7 36.0 reduce-scatter.4
where the time goes:
time: 580 us; the launch traced here: 579 us
  waiting for transfers between devices  357 us (62%)
  blocking collectives  103 us (18%)
  local copies, waits for them, and re-layouts  39.6 us (7%)
  matrix products  36.5 us (6%)
  other arithmetic  22.5 us (4%)
  between operations  14.9 us (3%)
    all_gather x1, waiting for transfers between devices, on_device(): lax.all_gather(up_weight, 'sp', axis=0, tiled=True)  127 us
    all_gather x1, waiting for transfers between devices, on_device(): lax.all_gather(down_weight, 'sp', axis=1, tiled=True)  113 us
    all_gather x3, blocking collectives, carried_in(): lax.all_gather(a.astype(kind), axis)  81.7 us
    reduce_scatter x1, waiting for transfers between devices, on_device(): lax.psum_scatter((jnp.dot(mixed_wide, output_wide, preferred_element_type...  52.4 us
    reduce_scatter x1, waiting for transfers between devices, on_device(): lax.psum_scatter(down_sum.astype(jnp.bfloat16), 'tp', scatter_dimension=0...  36.2 us
    all_gather x1, waiting for transfers between devices, on_device(): lax.all_gather(row_norm(middle, norm_gain), 'tp', axis=0, tiled=True)  27.1 us
    unnamed x1, blocking collectives  21.4 us
    dynamic_update_slice x18, local copies, waits for them, and re-layouts, local_group(): lax.scan(block_step, carried, (query_rot.reshape(blocks, BLOCK, count_of_...  21.1 us
  transfers between devices with their start and end apart: 5, of which 5 were waited for; matrix products, arithmetic and copies ran while one was open for 2% of the time, Pallas kernels for 0%

commit v1 on v0

--- a/solution.py
+++ b/solution.py
@@ -183,7 +183,7 @@
     hidden = jnp.square(jax.nn.relu(up_sum)).astype(jnp.bfloat16)
     down_sum = jnp.dot(
         hidden,
-        lax.all_gather(down_weight, "sp", axis=1, tiled=True),
+        jnp.concatenate(lax.all_gather(down_weight, "sp"), axis=1),
         preferred_element_type=jnp.float32,
     )
     down_rows = lax.psum_scatter(

time: 580 us -> 547 us (0.943)
  waiting for transfers between devices: 357 us -> 316 us
  local copies, waits for them, and re-layouts: 39.6 us -> 50.9 us
    all_gather x1, waiting for transfers between devices: 113 us -> 84.1 us  [on_device(): lax.all_gather(down_weight, 'sp')]
    reshape x0 -> x1, local copies, waits for them, and re-layouts: none -> 11.8 us  [on_device(): jnp.concatenate(lax.all_gather(down_weight, 'sp'), axis=1)]
    all_gather x1, waiting for transfers between devices: 27.1 us -> 16.2 us  [on_device(): lax.all_gather(row_norm(middle, norm_gain), 'tp', axis=0, tiled=True)]
  transfers between devices with their start and end apart: 5 -> 5, of which waited for: 5 -> 5; matrix products, arithmetic and copies ran while one was open for 2% -> 3% of each run, Pallas kernels for 0% -> 0%
where the time goes in v1:
time: 547 us; the launch traced here: 546 us
  waiting for transfers between devices  316 us (58%)
  blocking collectives  103 us (19%)
  local copies, waits for them, and re-layouts  50.9 us (9%)
  matrix products  31.2 us (6%)
  other arithmetic  22.5 us (4%)
  between operations  16.8 us (3%)
    all_gather x1, waiting for transfers between devices, on_device(): lax.all_gather(up_weight, 'sp', axis=0, tiled=True)  126 us
    all_gather x1, waiting for transfers between devices, on_device(): lax.all_gather(down_weight, 'sp')  84.1 us
    all_gather x3, blocking collectives, carried_in(): lax.all_gather(a.astype(kind), axis)  81.7 us
    reduce_scatter x1, waiting for transfers between devices, on_device(): lax.psum_scatter((jnp.dot(mixed_wide, output_wide, preferred_element_type...  52.4 us
    reduce_scatter x1, waiting for transfers between devices, on_device(): lax.psum_scatter(down_sum.astype(jnp.bfloat16), 'tp', scatter_dimension=0...  36.2 us
    unnamed x1, blocking collectives  21.4 us
    dynamic_update_slice x18, local copies, waits for them, and re-layouts, local_group(): lax.scan(block_step, carried, (query_rot.reshape(blocks, BLOCK, count_of_...  21.1 us
    all_gather x1, waiting for transfers between devices, on_device(): lax.all_gather(row_norm(middle, norm_gain), 'tp', axis=0, tiled=True)  16.2 us
  transfers between devices with their start and end apart: 5, of which 5 were waited for; matrix products, arithmetic and copies ran while one was open for 3% of the time, Pallas kernels for 0%

profile of v1, /device:TPU:0, one launch (start us, length us, event | category | flops | bytes accessed | tf_op | source)
XLA Modules:
  0.0 545.9 jit_solution(5329248149369825760)
XLA Ops:
  7.4 0.8 reduce.3
  9.0 1.1 copy.100
  10.1 1.1 copy.102
  12.8 25.0 %while.43 = (s32[]{:T(128)}, f32[2,64,64]{2,1,0:T(8,128)S(1)}, f32[6,128,2,64]{1,0,3,2:T(8,128)}, f32[6,128,2]{2,1,0:T(8,128)S(1)}, f32[6,128,2,64]{1,0,3,2:T(8,...) while((s32[]{:T(128)}, f32[2,64,64]{2,1,0:T(8,128)S(1)}, ...), condition=%wide.region_9.10_spmd.clone, body=%wide.region_7.9_spmd.clone.sunk | while | flops 12877827 | bytes 1099440 | solution.py:82
  13.9 2.8 dynamic_update_slice.14
  18.0 2.8 dynamic_update_slice.14
  22.2 2.8 dynamic_update_slice.14
  26.3 2.8 dynamic_update_slice.14
  30.5 2.8 dynamic_update_slice.14
  34.7 2.8 dynamic_update_slice.14
  37.7 34.6 %all-gather.1 = bf16[16,64,64]{2,1,0:T(8,128)(2,1)} all-gather(bf16[2,64,64]{2,1,0:T(8,128)(2,1)S(1)} %convert_element_type.115), channel_id=3, replica_groups=mesh['sp'=8,'tp'=4] {'sp'}, dimensions={0}, use_global_device_ids=true | all-gather | bytes 147456 | tf_op jit(solution)/shard_map/all_gather | solution.py:17
  72.3 1.0 reshape_reshape.16
  73.2 1.0 bitcast_convert_fusion.1
  74.2 1.9 fusion.74
  76.3 0.9 maximum_multiply_fusion.1
  77.2 27.8 %while.42 = (s32[]{:T(128)}, f32[1,128,128]{2,1,0:T(8,128)S(1)}, f32[6,128,1,128]{3,1,0,2:T(8,128)}, f32[6,128,1]{1,2,0:T(1,128)}, f32[6,128,1,128]{3,2,1,0:T(1,...) while((s32[]{:T(128)}, f32[1,128,128]{2,1,0:T(8,128)S(1)}, ...), condition=%wide.region_2.3_spmd.clone, body=%wide.region_0.2_spmd.clone.sunk | while | flops 17006596 | bytes 1515172 | solution.py:82
  77.2 0.7 fusion.149
  78.8 0.6 fusion.150
  81.9 0.7 fusion.149
  83.5 0.6 fusion.150
  86.5 0.7 fusion.149
  88.1 0.6 fusion.150
  91.1 0.7 fusion.149
  92.7 0.6 fusion.150
  95.7 0.7 fusion.149
  97.3 0.6 fusion.150
  100.4 0.7 fusion.149
  102.0 0.6 fusion.150
  103.5 0.6 constant_dynamic-update-slice_fusion.2
  105.0 30.9 %all-gather = bf16[8,128,128]{2,1,0:T(8,128)(2,1)S(1)} all-gather(bf16[1,128,128]{2,1,0:T(8,128)(2,1)S(1)} %convert_element_type.113), channel_id=2, replica_groups=mesh['sp'=8,'tp'=4] {'sp'}, dimensions={0}, use_global_device_ids=true | all-gather | bytes 294912 | tf_op jit(solution)/shard_map/all_gather | solution.py:17
  136.5 0.6 slice.73
  139.1 0.7 dynamic-update-slice
  139.8 21.4 %all-reduce = bf16[8]{0:T(256)(128)(2,1)S(1)} all-reduce(bf16[8]{0:T(256)(128)(2,1)S(1)} %dynamic-update-slice), channel_id=1, replica_groups=mesh['sp'=8,'tp'=4] {'sp'}, use_global_device_ids=true, to_apply=%add | all-reduce | flops 8 | bytes 32
  162.4 16.3 %all-gather.3 = bf16[8,1,2]{2,1,0:T(2,128)(2,1)S(1)} all-gather(bf16[1,1,2]{2,1,0:T(2,128)(2,1)S(1)} %bitcast.327), channel_id=1, replica_groups=mesh['sp'=8,'tp'=4] {'sp'}, dimensions={0}, use_global_device_ids=true | all-gather | bytes 36 | tf_op jit(solution)/shard_map/all_gather | solution.py:17
  178.8 1.2 reshape.616
  181.5 1.0 fusion.79
  182.5 2.8 add_convert_fusion
  186.0 52.4 %reduce-scatter.3.cloned.1.call-done = bf16[192,2048]{1,0:T(8,128)(2,1)} async-done(((bf16[768,2048]{1,0:T(8,128)(2,1)}), bf16[192,2048]{1,0:T(8,128)(2,1)}) %reduce-scatter.3.cloned.1.call-update) | async-done | bytes 786448 | tf_op jit(solution)/shard_map/reduce_scatter | solution.py:167
  238.4 1.5 fusion.47
  239.9 2.3 fusion.49
  243.1 84.1 %all-gather.12.cloned.1.call-done = bf16[16384,256]{1,0:T(8,128)(2,1)} async-done(((bf16[2048,256]{1,0:T(8,128)(2,1)}), bf16[16384,256]{1,0:T(8,128)(2,1)}) %all-gather.12.cloned.1.call-update) | async-done | bytes 8388624 | tf_op jit(solution)/shard_map/all_gather | solution.py:186
  327.2 11.8 %copy.112 = bf16[2048,8,256]{0,2,1:T(8,128)(2,1)} copy(bf16[2048,8,256]{2,0,1:T(8,128)(2,1)} %bitcast.300) | data formatting | bytes 16777216 | tf_op jit(solution)/shard_map/reshape | solution.py:186
  339.1 16.2 %all-gather.8.cloned.1.call-done = bf16[768,2048]{1,0:T(8,128)(2,1)} async-done(((bf16[192,2048]{1,0:T(8,128)(2,1)}), bf16[768,2048]{1,0:T(8,128)(2,1)}) %all-gather.8.cloned.1.call-update) | async-done | bytes 3145744 | tf_op jit(solution)/shard_map/all_gather | solution.py:177
  355.2 126.2 %all-gather.10.cloned.1.call-done = bf16[2048,2048]{1,0:T(8,128)(2,1)} async-done(((bf16[256,2048]{1,0:T(8,128)(2,1)}), bf16[2048,2048]{1,0:T(8,128)(2,1)}) %all-gather.10.cloned.1.call-update) | async-done | bytes 8388624 | tf_op jit(solution)/shard_map/all_gather | solution.py:180
  481.4 10.2 %multiply_convert_fusion = bf16[768,2048]{1,0:T(8,128)(2,1)S(1)} fusion(bf16[768,2048]{1,0:T(8,128)(2,1)} %all-gather.8.cloned.1.call-done, bf16[2048,2048]{1,0:T(8,128)(2,1)} %all-gather.10.cloned.1.call-done), kind=kOutput, calls=%fused_computation.73 | convolution fusion | flops 6447169536 | bytes 14680064 | tf_op jit(solution)/shard_map/dot_general | solution.py:178
  491.6 8.1 %convolution_convert_fusion = bf16[768,2048]{1,0:T(8,128)(2,1)} fusion(bf16[768,2048]{1,0:T(8,128)(2,1)S(1)} %multiply_convert_fusion, bf16[2048,2048]{0,1:T(8,128)(2,1)S(1)} %bitcast.301), kind=kOutput, calls=%fused_computation.75 | convolution fusion | flops 6444023808 | bytes 14680064 | tf_op jit(solution)/shard_map/dot_general | solution.py:184
  499.8 36.2 %reduce-scatter.5.cloned.1.call-done = bf16[192,2048]{1,0:T(8,128)(2,1)} async-done(((bf16[768,2048]{1,0:T(8,128)(2,1)}), bf16[192,2048]{1,0:T(8,128)(2,1)}) %reduce-scatter.5.cloned.1.call-update) | async-done | bytes 786448 | tf_op jit(solution)/shard_map/reduce_scatter | solution.py:189
  536.0 2.4 fusion.50
  (236 shorter events, 30.4 us)
Async XLA Ops:
  7.4 174.1 %copy-start = (bf16[128,2048]{1,0:T(8,128)(2,1)S(1)}, bf16[128,2048]{1,0:T(8,128)(2,1)}, u32[]{:S(2)}) copy-start(bf16[128,2048]{1,0:T(8,128)(2,1)} %param.33) | copy-start | bytes 1572868
  7.4 4.5 copy-start.9
  7.4 231.1 %reduce-scatter.3.cloned.1.call-start = ((), (), s32[]{:S(2)}) async-start(), calls=%async_computation.2 | async-start | bytes 3932160 | tf_op jit(solution)/shard_map/reduce_scatter | solution.py:167
  10.1 2.3 copy-start.10
  12.7 60.5 %copy-start.6 = (bf16[768,128]{1,0:T(8,128)(2,1)S(1)}, bf16[768,128]{1,0:T(8,128)(2,1)}, u32[]{:S(2)}) copy-start(bf16[768,128]{1,0:T(8,128)(2,1)} %param.23) | copy-start | bytes 589828
  77.2 61.3 %copy-start.12 = (u32[32]{0:T(128)S(1)}, u32[32]{0:T(128)}, u32[]{:S(2)}) copy-start(u32[32]{0:T(128)} %constant.123) | copy-start | bytes 388
  105.0 75.4 %copy-start.7 = (bf16[768,128]{1,0:T(8,128)(2,1)S(1)}, bf16[768,128]{1,0:T(8,128)(2,1)}, u32[]{:S(2)}) copy-start(bf16[768,128]{1,0:T(8,128)(2,1)} %param.31) | copy-start | bytes 589828
  105.0 75.6 %copy-start.5 = (f32[6,128,1,128]{3,1,0,2:T(8,128)S(1)}, f32[6,128,1,128]{3,1,0,2:T(8,128)}, u32[]{:S(2)}) copy-start(f32[6,128,1,128]{3,1,0,2:T(8,128)} %get-tuple-element.151) | copy-start | bytes 1179652
  178.8 2.4 copy-start.8
  181.5 1.0 copy-start.4
  185.3 0.7 copy-start.11
  185.3 53.1 %copy-start.2 = (bf16[192,2048]{1,0:T(8,128)(2,1)S(1)}, bf16[192,2048]{1,0:T(8,128)(2,1)}, u32[]{:S(2)}) copy-start(bf16[192,2048]{1,0:T(8,128)(2,1)} %param.22) | copy-start | bytes 2359300
  185.3 141.9 %all-gather.12.cloned.1.call-start = ((), (), s32[]{:S(2)}) async-start(), calls=%async_computation.6 | async-start | bytes 9437184 | tf_op jit(solution)/shard_map/all_gather | solution.py:186
  185.9 169.3 %all-gather.8.cloned.1.call-start = ((), (), s32[]{:S(2)}) async-start(), calls=%async_computation.3 | async-start | bytes 3932160 | tf_op jit(solution)/shard_map/all_gather | solution.py:177
  242.3 239.2 %all-gather.10.cloned.1.call-start = ((), (), s32[]{:S(2)}) async-start(), calls=%async_computation.4 | async-start | bytes 9437184 | tf_op jit(solution)/shard_map/all_gather | solution.py:180
  242.8 293.1 %reduce-scatter.5.cloned.1.call-start = ((), (), s32[]{:S(2)}) async-start(), calls=%async_computation.5 | async-start | bytes 3932160 | tf_op jit(solution)/shard_map/reduce_scatter | solution.py:189
  481.4 10.2 %copy-start.1 = (bf16[2048,8,256]{0,2,1:T(8,128)(2,1)S(1)}, bf16[2048,8,256]{0,2,1:T(8,128)(2,1)}, u32[]{:S(2)}) copy-start(bf16[2048,8,256]{0,2,1:T(8,128)(2,1)} %copy.112) | copy-start | bytes 25165828
  499.7 36.2 %copy-start.3 = (bf16[192,2048]{1,0:T(8,128)(2,1)S(1)}, bf16[192,2048]{1,0:T(8,128)(2,1)}, u32[]{:S(2)}) copy-start(bf16[192,2048]{1,0:T(8,128)(2,1)} %reduce-scatter.3.cloned.1.call-done) | copy-start | bytes 2359300
Sparse Core Ops, SparseCore 0:
  185.5 52.9 reduce-scatter.2
  499.9 36.0 reduce-scatter.4
Sparse Core Ops, SparseCore 1:
  188.0 139.2 all-gather.11
  328.7 26.5 all-gather.7
  357.2 124.1 all-gather.9
